TPU v7x, 32 devices: a whole 2x2x4 slice. The times are simulated.
32 devices in a mesh: fs: 8 (over z, y), tp: 4 (over x, core).
Axes of the slice: x: 2, y: 2, z: 4, core: 2. Of those that a mesh axis runs over, the one named last changes fastest.
Arguments:
- x_saved: bfloat16 [16384, 2048], P('fs'), may hold values from -6 to 6
- h_saved: bfloat16 [16384, 1024], P('fs', 'tp'), may hold values from -6 to 6
- key_cot: bfloat16 [16384, 1024], P('fs', 'tp'), may hold values from -6 to 6
- value_cot: bfloat16 [16384, 1024], P('fs', 'tp'), may hold values from -6 to 6
- out_cot: bfloat16 [16384, 2048], P('fs'), may hold values from -6 to 6
- w_key: float32 [2048, 1024], P('fs', 'tp'), may hold values from -0.125 to 0.125
- w_value: float32 [2048, 1024], P('fs', 'tp'), may hold values from -0.125 to 0.125
- w_out: float32 [1024, 2048], P('tp', 'fs'), may hold values from -0.1875 to 0.1875
- p_key: bfloat16 [2048, 256], P('fs'), may hold values from -1 to 1, as said below
- p_value: bfloat16 [2048, 256], P('fs'), may hold values from -1 to 1, as said below
- p_out: bfloat16 [2048, 256], P('fs'), may hold values from -1 to 1, as said below
- m_key: float32 [2, 256, 1024], P(None, 'fs', 'tp'), may hold values from -1.5 to 1.5, as said below
- m_value: float32 [2, 256, 1024], P(None, 'fs', 'tp'), may hold values from -1.5 to 1.5, as said below
- m_out: float32 [2, 256, 1024], P(None, 'fs', 'tp'), may hold values from -1.5 to 1.5, as said below
Outputs:
- step_key: float32 [2048, 1024], P('fs', 'tp')
- step_value: float32 [2048, 1024], P('fs', 'tp')
- step_out: float32 [1024, 2048], P('tp', 'fs')
- copy_key: bfloat16 [2048, 1024], P(None, 'tp')
- copy_value: bfloat16 [2048, 1024], P(None, 'tp')
- copy_out: bfloat16 [1024, 2048], P('tp')
- new_m_key: float32 [2, 256, 1024], P(None, 'fs', 'tp')
- new_m_value: float32 [2, 256, 1024], P(None, 'fs', 'tp')
- new_m_out: float32 [2, 256, 1024], P(None, 'fs', 'tp')
Inputs may be any that keep to these rules, and one draw needn't show every extreme that they name: `p_key`: factor entries are real-valued, dense and of full rank. `p_value`: factor entries are real-valued, dense and of full rank. `p_out`: factor entries are real-valued, dense and of full rank. `m_key`: plane 1 (second moments) lies in 0.05 to 1. `m_value`: plane 1 (second moments) lies in 0.05 to 1. `m_out`: plane 1 (second moments) lies in 0.05 to 1.
All inputs are finite; a program needn't handle non-finite values.
Results may differ from a plain program's by a relative error of at most 0.0085.
Values may be sent and summed in bfloat16 or wider, within the bound.
A program may use at most 128 MiB of HBM per device.

v0:
```python
import jax
import jax.numpy as jnp
from jax import lax
from jax.sharding import PartitionSpec as P

beta_one = 0.9
beta_two = 0.9
learn_rate = 0.01


def project_rows(factors, grads, local_width):
    high_part = grads.astype(jnp.bfloat16)
    low_part = (grads - high_part.astype(jnp.float32)).astype(jnp.bfloat16)
    outputs = []
    for member in range(3):
        lower = member * local_width
        upper = (member + 1) * local_width
        factor_t = factors[member].T
        first_term = jnp.dot(
            factor_t, high_part[:, lower:upper], preferred_element_type=jnp.float32
        )
        second_term = jnp.dot(
            factor_t, low_part[:, lower:upper], preferred_element_type=jnp.float32
        )
        outputs.append(first_term + second_term)
    return jnp.concatenate(outputs, axis=1)


def body(
    x_saved,
    h_saved,
    key_cot,
    value_cot,
    out_cot,
    w_key,
    w_value,
    w_out,
    p_key,
    p_value,
    p_out,
    m_key,
    m_value,
    m_out,
):
    local_width = key_cot.shape[1]
    x_cols = x_saved.T
    y_cols = out_cot.T
    grad_k = jnp.dot(x_cols, key_cot, preferred_element_type=jnp.float32)
    grad_v = jnp.dot(x_cols, value_cot, preferred_element_type=jnp.float32)
    grad_o = jnp.dot(y_cols, h_saved, preferred_element_type=jnp.float32)
    whole_grad = jnp.concatenate([grad_k, grad_v, grad_o], axis=1)
    partial_value = project_rows(
        (
            lax.all_gather(p_key, "fs", axis=0, tiled=True),
            lax.all_gather(p_value, "fs", axis=0, tiled=True),
            lax.all_gather(p_out, "fs", axis=0, tiled=True),
        ),
        whole_grad,
        local_width,
    )
    projected = lax.psum_scatter(partial_value, "fs", scatter_dimension=0, tiled=True)
    total = lax.psum(jnp.sum(projected * projected), ("fs", "tp"))
    entries = projected.size * lax.axis_size("fs") * lax.axis_size("tp")
    normed = projected / jnp.sqrt(total / entries + 1e-06)
    moments = jnp.concatenate([m_key, m_value, m_out], axis=2)
    moment_one = beta_one * moments[0] + (1 - beta_one) * normed
    moment_two = beta_two * moments[1] + (1 - beta_two) * normed * normed
    direction = (moment_one / jnp.sqrt(moment_two)).astype(jnp.bfloat16)
    gathered = lax.all_gather(direction, "fs", axis=0, tiled=True)
    step_key = jnp.dot(p_key, gathered[:, :local_width], preferred_element_type=jnp.float32)
    step_value = jnp.dot(
        p_value, gathered[:, local_width : 2 * local_width], preferred_element_type=jnp.float32
    )
    step_out = jnp.dot(p_out, gathered[:, 2 * local_width :], preferred_element_type=jnp.float32).T
    fresh_key = (w_key - learn_rate * step_key).astype(jnp.bfloat16)
    fresh_value = (w_value - learn_rate * step_value).astype(jnp.bfloat16)
    fresh_out = (w_out - learn_rate * step_out).astype(jnp.bfloat16)
    copy_key, copy_value, copy_out = (
        lax.all_gather(fresh_key, "fs", axis=0, tiled=True),
        lax.all_gather(fresh_value, "fs", axis=0, tiled=True),
        lax.all_gather(fresh_out, "fs", axis=1, tiled=True),
    )
    stacked = jnp.stack([moment_one, moment_two])
    new_m_key = stacked[:, :, :local_width]
    new_m_value = stacked[:, :, local_width : 2 * local_width]
    new_m_out = stacked[:, :, 2 * local_width :]
    return (
        step_key,
        step_value,
        step_out,
        copy_key,
        copy_value,
        copy_out,
        new_m_key,
        new_m_value,
        new_m_out,
    )


def solution(mesh):
    in_specs = (
        P("fs", None),
        P("fs", "tp"),
        P("fs", "tp"),
        P("fs", "tp"),
        P("fs", None),
        P("fs", "tp"),
        P("fs", "tp"),
        P("tp", "fs"),
        P("fs", None),
        P("fs", None),
        P("fs", None),
        P(None, "fs", "tp"),
        P(None, "fs", "tp"),
        P(None, "fs", "tp"),
    )
    out_specs = (
        P("fs", "tp"),
        P("fs", "tp"),
        P("tp", "fs"),
        P(None, "tp"),
        P(None, "tp"),
        P("tp", None),
        P(None, "fs", "tp"),
        P(None, "fs", "tp"),
        P(None, "fs", "tp"),
    )
    return jax.shard_map(body, mesh=mesh, in_specs=in_specs, out_specs=out_specs, check_vma=False)
```

profile of v0, /device:TPU:0, one launch (start us, length us, event | category | flops | bytes accessed | tf_op | source)
XLA Modules:
  0.0 409.5 jit_solution(15238596800766914783)
XLA Ops:
  9.5 5.9 %fusion.23 = f32[2048,256]{0,1:T(8,128)S(1)} fusion(bf16[2048,2048]{1,0:T(8,128)(2,1)} %param.14, bf16[2048,256]{1,0:T(8,128)(2,1)S(1)} %copy-done), kind=kOutput, calls=%fused_computation.47 | convolution fusion | flops 2147483648 | bytes 11534336 | tf_op jit(solution)/shard_map/dot_general | solution.py:48
  15.4 5.9 %fusion.24 = f32[2048,256]{0,1:T(8,128)S(1)} fusion(bf16[2048,2048]{1,0:T(8,128)(2,1)} %param.14, bf16[2048,256]{1,0:T(8,128)(2,1)S(1)} %copy-done.6), kind=kOutput, calls=%fused_computation.48 | convolution fusion | flops 2147483648 | bytes 11534336 | tf_op jit(solution)/shard_map/dot_general | solution.py:49
  21.4 2.4 fusion.25
  23.8 2.0 fusion
  25.8 2.1 subtract_convert_fusion
  27.8 25.3 %all-gather.7.cloned.1.call-done = bf16[2048,256]{1,0:T(8,128)(2,1)} async-done(((bf16[256,256]{1,0:T(8,128)(2,1)}), bf16[2048,256]{1,0:T(8,128)(2,1)}) %all-gather.7.cloned.1.call-update) | async-done | bytes 1048592 | tf_op jit(solution)/shard_map/all_gather | solution.py:54
  53.2 2.1 fusion.11
  55.2 39.1 %all-gather.9.cloned.1.call-done = bf16[2048,256]{1,0:T(8,128)(2,1)} async-done(((bf16[256,256]{1,0:T(8,128)(2,1)}), bf16[2048,256]{1,0:T(8,128)(2,1)}) %all-gather.9.cloned.1.call-update) | async-done | bytes 1048592 | tf_op jit(solution)/shard_map/all_gather | solution.py:55
  94.3 2.1 fusion.8
  98.1 1.7 fusion.2
  99.7 35.7 %all-gather.11.cloned.1.call-done = bf16[2048,256]{1,0:T(8,128)(2,1)} async-done(((bf16[256,256]{1,0:T(8,128)(2,1)}), bf16[2048,256]{1,0:T(8,128)(2,1)}) %all-gather.11.cloned.1.call-update) | async-done | bytes 1048592 | tf_op jit(solution)/shard_map/all_gather | solution.py:56
  135.5 2.0 fusion.5
  137.5 2.0 fusion.1
  141.2 61.6 %reduce-scatter.4.cloned.1.call-done = f32[32,768]{1,0:T(8,128)} async-done(((f32[256,768]{1,0:T(8,128)}), f32[32,768]{1,0:T(8,128)}) %reduce-scatter.4.cloned.1.call-update) | async-done | bytes 98320
  204.8 40.2 %psum.7 = f32[]{:T(128)} all-reduce(f32[]{:T(128)} %multiply_reduce_fusion), channel_id=1, replica_groups=mesh['fs'=8,'tp'=4] {'fs','tp'}, use_global_device_ids=true, to_apply=%region_2.0 | all-reduce | flops 1 | bytes 8 | tf_op jit(solution)/shard_map/psum | solution.py:62
  245.9 31.0 %all_gather.24 = bf16[256,768]{1,0:T(8,128)(2,1)S(1)} all-gather(bf16[32,768]{1,0:T(8,128)(2,1)S(1)} %copy.40), channel_id=1, replica_groups=mesh['fs'=8,'tp'=4] {'fs'}, dimensions={0}, use_global_device_ids=true | all-gather | bytes 442368 | tf_op jit(solution)/shard_map/all_gather | solution.py:69
  280.0 1.8 subtract_convert_fusion.2
  283.0 1.8 subtract_convert_fusion.3
  287.4 31.3 %all-gather.17.cloned.1.call-done = bf16[256,2048]{0,1:T(8,128)(2,1)} async-done(((bf16[256,256]{0,1:T(8,128)(2,1)}), bf16[256,2048]{0,1:T(8,128)(2,1)}) %all-gather.17.cloned.1.call-update) | async-done | bytes 1048592 | tf_op jit(solution)/shard_map/all_gather | solution.py:81
  318.8 2.3 copy.51
  321.0 38.4 %all-gather.15.cloned.1.call-done = bf16[2048,256]{0,1:T(8,128)(2,1)} async-done(((bf16[256,256]{0,1:T(8,128)(2,1)}), bf16[2048,256]{0,1:T(8,128)(2,1)}) %all-gather.15.cloned.1.call-update) | async-done | bytes 1048592 | tf_op jit(solution)/shard_map/all_gather | solution.py:80
  359.4 2.3 copy.50
  361.6 38.8 %all-gather.13.cloned.1.call-done = bf16[2048,256]{0,1:T(8,128)(2,1)} async-done(((bf16[256,256]{0,1:T(8,128)(2,1)}), bf16[2048,256]{0,1:T(8,128)(2,1)}) %all-gather.13.cloned.1.call-update) | async-done | bytes 1048592 | tf_op jit(solution)/shard_map/all_gather | solution.py:79
  400.4 2.3 copy.49
  (63 shorter events, 14.6 us)
Async XLA Ops:
  7.2 2.3 copy-start
  7.2 46.0 %all-gather.7.cloned.1.call-start = ((), (), s32[]{:S(2)}) async-start(), calls=%async_computation.1 | async-start | bytes 1179648 | tf_op jit(solution)/shard_map/all_gather | solution.py:54
  7.9 86.4 %all-gather.9.cloned.1.call-start = ((), (), s32[]{:S(2)}) async-start(), calls=%async_computation.2 | async-start | bytes 1179648 | tf_op jit(solution)/shard_map/all_gather | solution.py:55
  8.7 126.8 %all-gather.11.cloned.1.call-start = ((), (), s32[]{:S(2)}) async-start(), calls=%async_computation.3 | async-start | bytes 1179648 | tf_op jit(solution)/shard_map/all_gather | solution.py:56
  9.4 6.0 %copy-start.6 = (bf16[2048,256]{1,0:T(8,128)(2,1)S(1)}, bf16[2048,256]{1,0:T(8,128)(2,1)}, u32[]{:S(2)}) copy-start(bf16[2048,256]{1,0:T(8,128)(2,1)} %param.17) | copy-start | bytes 3145732
  9.4 193.5 %reduce-scatter.4.cloned.1.call-start = ((), (), s32[]{:S(2)}) async-start(), calls=%async_computation.7 | async-start | bytes 884736
  9.5 11.9 %slice-start = ((s8[8388608]{0:T(1024)(128)(4,1)}), s8[4194304]{0:T(1024)(128)(4,1)S(1)}, s32[]{:S(2)}) async-start(s8[8388608]{0:T(1024)(128)(4,1)} %bitcast.42), calls=%async_computation.8 | async-start | bytes 8388608
  15.4 5.9 %slice-start.1 = ((s8[8388608]{0:T(1024)(128)(4,1)}), s8[4194304]{0:T(1024)(128)(4,1)S(1)}, s32[]{:S(2)}) async-start(s8[8388608]{0:T(1024)(128)(4,1)} %bitcast.42), calls=%async_computation.9 | async-start | bytes 8388608
  15.4 5.9 %copy-start.7 = (bf16[2048,256]{1,0:T(8,128)(2,1)S(1)}, bf16[2048,256]{1,0:T(8,128)(2,1)}, u32[]{:S(2)}) copy-start(bf16[2048,256]{1,0:T(8,128)(2,1)} %param.15) | copy-start | bytes 3145732
  53.2 43.2 %copy-start.8 = (bf16[2048,256]{1,0:T(8,128)(2,1)S(1)}, bf16[2048,256]{1,0:T(8,128)(2,1)}, u32[]{:S(2)}) copy-start(bf16[2048,256]{1,0:T(8,128)(2,1)} %all-gather.7.cloned.1.call-done) | copy-start | bytes 3145732
  94.3 3.8 copy-start.9
  137.4 3.4 copy-start.3
  137.5 3.4 copy-start.4
  137.5 3.4 copy-start.5
  139.5 65.1 %copy-start.2 = (f32[256,256]{1,0:T(8,128)S(1)}, f32[256,256]{1,0:T(8,128)}, u32[]{:S(2)}) copy-start(f32[256,256]{1,0:T(8,128)} %param.21) | copy-start | bytes 786436
  140.8 178.0 %all-gather.17.cloned.1.call-start = ((), (), s32[]{:S(2)}) async-start(), calls=%async_computation.6 | async-start | bytes 1179648 | tf_op jit(solution)/shard_map/all_gather | solution.py:81
  278.0 8.7 %copy-start.1 = (f32[256,256]{1,0:T(8,128)}, f32[256,256]{1,0:T(8,128)S(1)}, u32[]{:S(2)}) copy-start(f32[256,256]{1,0:T(8,128)S(1)} %fusion.14) | copy-start | bytes 786436
  278.9 80.5 %all-gather.15.cloned.1.call-start = ((), (), s32[]{:S(2)}) async-start(), calls=%async_computation.5 | async-start | bytes 1179648 | tf_op jit(solution)/shard_map/all_gather | solution.py:80
  281.8 118.6 %all-gather.13.cloned.1.call-start = ((), (), s32[]{:S(2)}) async-start(), calls=%async_computation.4 | async-start | bytes 1179648 | tf_op jit(solution)/shard_map/all_gather | solution.py:79
Sparse Core Ops, SparseCore 0:
  10.1 42.9 all-gather.6
  55.3 38.9 all-gather.8
  96.4 38.9 all-gather.10
  140.9 61.9 reduce-scatter.3
  279.0 39.7 all-gather.16
  321.2 38.0 all-gather.14
  362.0 38.3 all-gather.12
where the time goes:
time: 410 us
  waiting for transfers between devices  272 us (66%)
  blocking collectives  71.1 us (17%)
  matrix products  30.3 us (7%)
  between operations  15.2 us (4%)
  local copies, waits for them, and re-layouts  13.9 us (3%)
  other arithmetic  6.34 us (2%)
    unnamed x8, waiting for transfers between devices  63.8 us
    psum x1, blocking collectives, body(): total = lax.psum(jnp.sum(projected * projected), ('fs', 'tp'))  40.2 us
    all_gather x1, waiting for transfers between devices, body(): lax.all_gather(p_value, 'fs', axis=0, tiled=True)  39.1 us
    all_gather x1, waiting for transfers between devices, body(): lax.all_gather(fresh_key, 'fs', axis=0, tiled=True)  38.8 us
    all_gather x1, waiting for transfers between devices, body(): lax.all_gather(fresh_value, 'fs', axis=0, tiled=True)  38.4 us
    all_gather x1, waiting for transfers between devices, body(): lax.all_gather(p_out, 'fs', axis=0, tiled=True)  35.7 us
    all_gather x1, waiting for transfers between devices, body(): lax.all_gather(fresh_out, 'fs', axis=1, tiled=True)  31.3 us
    all_gather x1, blocking collectives, body(): gathered = lax.all_gather(direction, 'fs', axis=0, tiled=True)  31 us
  transfers between devices with their start and end apart: 7, of which 7 were waited for; matrix products, arithmetic and copies ran while one was open for 10% of the time, Pallas kernels for 0%

commit v1 on v0

--- a/solution.py
+++ b/solution.py
@@ -66,7 +66,14 @@
     moment_one = beta_one * moments[0] + (1 - beta_one) * normed
     moment_two = beta_two * moments[1] + (1 - beta_two) * normed * normed
     direction = (moment_one / jnp.sqrt(moment_two)).astype(jnp.bfloat16)
-    gathered = lax.all_gather(direction, "fs", axis=0, tiled=True)
+    count = lax.axis_size("fs")
+    right = [(i, (i + 1) % count) for i in range(count)]
+    blocks = [direction]
+    for reach in range(1, count):
+        blocks = [lax.ppermute(blocks[0], "fs", right), *blocks]
+    whole = jnp.concatenate(blocks, axis=0)
+    turn = (lax.axis_index("fs") + 1) * blocks[-1].shape[0]
+    gathered = jnp.roll(whole, turn, axis=0)
     step_key = jnp.dot(p_key, gathered[:, :local_width], preferred_element_type=jnp.float32)
     step_value = jnp.dot(
         p_value, gathered[:, local_width : 2 * local_width], preferred_element_type=jnp.float32

time: 410 us -> 446 us (1.088)
  waiting for transfers between devices: 272 us -> 330 us
  blocking collectives: 71.1 us -> 40.1 us
  local copies, waits for them, and re-layouts: 13.9 us -> 19.8 us
    ppermute x0 -> x7, waiting for transfers between devices: none -> 58.4 us  [body(): blocks = [lax.ppermute(blocks[0], 'fs', right), *blocks]]
    all_gather x1 -> x0, blocking collectives: 31 us -> none  [body(): gathered = lax.all_gather(direction, 'fs', axis=0, tiled=True)]
    unnamed x38 -> x44, local copies, waits for them, and re-layouts: 13.4 us -> 15.5 us
  transfers between devices with their start and end apart: 7 -> 14, of which waited for: 7 -> 14; matrix products, arithmetic and copies ran while one was open for 10% -> 9% of each run, Pallas kernels for 0% -> 0%
where the time goes in v1:
time: 446 us; the launch traced here: 445 us
  waiting for transfers between devices  330 us (74%)
  blocking collectives  40.1 us (9%)
  matrix products  29.6 us (7%)
  local copies, waits for them, and re-layouts  19.8 us (4%)
  between operations  15.2 us (3%)
  other arithmetic  7.29 us (2%)
    unnamed x8, waiting for transfers between devices  63.9 us
    ppermute x7, waiting for transfers between devices, body(): blocks = [lax.ppermute(blocks[0], 'fs', right), *blocks]  58.4 us
    psum x1, blocking collectives, body(): total = lax.psum(jnp.sum(projected * projected), ('fs', 'tp'))  40.1 us
    all_gather x1, waiting for transfers between devices, body(): lax.all_gather(p_value, 'fs', axis=0, tiled=True)  39.1 us
    all_gather x1, waiting for transfers between devices, body(): lax.all_gather(fresh_key, 'fs', axis=0, tiled=True)  38.8 us
    all_gather x1, waiting for transfers between devices, body(): lax.all_gather(fresh_value, 'fs', axis=0, tiled=True)  38.4 us
    all_gather x1, waiting for transfers between devices, body(): lax.all_gather(p_out, 'fs', axis=0, tiled=True)  35.7 us
    all_gather x1, waiting for transfers between devices, body(): lax.all_gather(fresh_out, 'fs', axis=1, tiled=True)  30.6 us
  transfers between devices with their start and end apart: 14, of which 14 were waited for; matrix products, arithmetic and copies ran while one was open for 9% of the time, Pallas kernels for 0%

profile of v1, /device:TPU:0, one launch (start us, length us, event | category | flops | bytes accessed | tf_op | source)
XLA Modules:
  0.0 444.9 jit_solution(16958204833958219884)
XLA Ops:
  9.5 5.8 %fusion.24 = f32[2048,256]{0,1:T(8,128)S(1)} fusion(bf16[2048,2048]{1,0:T(8,128)(2,1)} %param.14, bf16[2048,256]{1,0:T(8,128)(2,1)S(1)} %copy-done), kind=kOutput, calls=%fused_computation.48 | convolution fusion | flops 2147483648 | bytes 11534336 | tf_op jit(solution)/shard_map/dot_general | solution.py:48
  15.3 5.9 %fusion.25 = f32[2048,256]{0,1:T(8,128)S(1)} fusion(bf16[2048,2048]{1,0:T(8,128)(2,1)} %param.14, bf16[2048,256]{1,0:T(8,128)(2,1)S(1)} %copy-done.11), kind=kOutput, calls=%fused_computation.49 | convolution fusion | flops 2147483648 | bytes 11534336 | tf_op jit(solution)/shard_map/dot_general | solution.py:49
  21.4 2.4 fusion.26
  25.8 2.1 subtract_convert_fusion
  27.9 25.3 %all-gather.7.cloned.1.call-done = bf16[2048,256]{1,0:T(8,128)(2,1)} async-done(((bf16[256,256]{1,0:T(8,128)(2,1)}), bf16[2048,256]{1,0:T(8,128)(2,1)}) %all-gather.7.cloned.1.call-update) | async-done | bytes 1048592 | tf_op jit(solution)/shard_map/all_gather | solution.py:54
  55.2 39.1 %all-gather.9.cloned.1.call-done = bf16[2048,256]{1,0:T(8,128)(2,1)} async-done(((bf16[256,256]{1,0:T(8,128)(2,1)}), bf16[2048,256]{1,0:T(8,128)(2,1)}) %all-gather.9.cloned.1.call-update) | async-done | bytes 1048592 | tf_op jit(solution)/shard_map/all_gather | solution.py:55
  99.7 35.7 %all-gather.11.cloned.1.call-done = bf16[2048,256]{1,0:T(8,128)(2,1)} async-done(((bf16[256,256]{1,0:T(8,128)(2,1)}), bf16[2048,256]{1,0:T(8,128)(2,1)}) %all-gather.11.cloned.1.call-update) | async-done | bytes 1048592 | tf_op jit(solution)/shard_map/all_gather | solution.py:56
  141.1 61.8 %reduce-scatter.4.cloned.1.call-done = f32[32,768]{1,0:T(8,128)} async-done(((f32[256,768]{1,0:T(8,128)}), f32[32,768]{1,0:T(8,128)}) %reduce-scatter.4.cloned.1.call-update) | async-done | bytes 98320
  204.8 40.1 %psum.7 = f32[]{:T(128)} all-reduce(f32[]{:T(128)} %multiply_reduce_fusion), channel_id=1, replica_groups=mesh['fs'=8,'tp'=4] {'fs','tp'}, use_global_device_ids=true, to_apply=%region_2.0 | all-reduce | flops 1 | bytes 8 | tf_op jit(solution)/shard_map/psum | solution.py:62
  245.7 2.5 collective-permute-start
  248.3 6.2 %collective-permute-done = bf16[32,768]{0,1:T(8,128)(2,1)S(1)} collective-permute-done((bf16[32,768]{0,1:T(8,128)(2,1)S(1)}, bf16[32,768]{0,1:T(8,128)(2,1)S(1)}, u32[]{:S(2)}, u32[]{:S(2)}) %collective-permute-start) | collective-permute-done | bytes 49184 | tf_op jit(solution)/shard_map/ppermute | solution.py:73
  254.5 8.4 %collective-permute-done.1 = bf16[32,768]{0,1:T(8,128)(2,1)S(1)} collective-permute-done((bf16[32,768]{0,1:T(8,128)(2,1)S(1)}, bf16[32,768]{0,1:T(8,128)(2,1)S(1)}, u32[]{:S(2)}, u32[]{:S(2)}) %collective-permute-start.1) | collective-permute-done | bytes 49184 | tf_op jit(solution)/shard_map/ppermute | solution.py:73
  262.9 8.4 %collective-permute-done.2 = bf16[32,768]{0,1:T(8,128)(2,1)S(1)} collective-permute-done((bf16[32,768]{0,1:T(8,128)(2,1)S(1)}, bf16[32,768]{0,1:T(8,128)(2,1)S(1)}, u32[]{:S(2)}, u32[]{:S(2)}) %collective-permute-start.2) | collective-permute-done | bytes 49184 | tf_op jit(solution)/shard_map/ppermute | solution.py:73
  271.2 8.4 %collective-permute-done.3 = bf16[32,768]{0,1:T(8,128)(2,1)S(1)} collective-permute-done((bf16[32,768]{0,1:T(8,128)(2,1)S(1)}, bf16[32,768]{0,1:T(8,128)(2,1)S(1)}, u32[]{:S(2)}, u32[]{:S(2)}) %collective-permute-start.3) | collective-permute-done | bytes 49184 | tf_op jit(solution)/shard_map/ppermute | solution.py:73
  279.6 9.3 %collective-permute-done.4 = bf16[32,768]{0,1:T(8,128)(2,1)S(1)} collective-permute-done((bf16[32,768]{0,1:T(8,128)(2,1)S(1)}, bf16[32,768]{0,1:T(8,128)(2,1)S(1)}, u32[]{:S(2)}, u32[]{:S(2)}) %collective-permute-start.4) | collective-permute-done | bytes 49184 | tf_op jit(solution)/shard_map/ppermute | solution.py:73
  288.9 10.5 %collective-permute-done.5 = bf16[32,768]{0,1:T(8,128)(2,1)S(1)} collective-permute-done((bf16[32,768]{0,1:T(8,128)(2,1)S(1)}, bf16[32,768]{0,1:T(8,128)(2,1)S(1)}, u32[]{:S(2)}, u32[]{:S(2)}) %collective-permute-start.5) | collective-permute-done | bytes 49184 | tf_op jit(solution)/shard_map/ppermute | solution.py:73
  300.6 7.3 %collective-permute-done.6 = bf16[32,768]{0,1:T(8,128)(2,1)} collective-permute-done((bf16[32,768]{0,1:T(8,128)(2,1)S(1)}, bf16[32,768]{0,1:T(8,128)(2,1)}, u32[]{:S(2)}, u32[]{:S(2)}) %collective-permute-start.6) | collective-permute-done | bytes 49184 | tf_op jit(solution)/shard_map/ppermute | solution.py:73
  307.9 3.2 concatenate.18
  323.5 30.6 %all-gather.17.cloned.1.call-done = bf16[256,2048]{0,1:T(8,128)(2,1)} async-done(((bf16[256,256]{0,1:T(8,128)(2,1)}), bf16[256,2048]{0,1:T(8,128)(2,1)}) %all-gather.17.cloned.1.call-update) | async-done | bytes 1048592 | tf_op jit(solution)/shard_map/all_gather | solution.py:88
  354.1 2.3 copy.50
  356.4 38.4 %all-gather.15.cloned.1.call-done = bf16[2048,256]{0,1:T(8,128)(2,1)} async-done(((bf16[256,256]{0,1:T(8,128)(2,1)}), bf16[2048,256]{0,1:T(8,128)(2,1)}) %all-gather.15.cloned.1.call-update) | async-done | bytes 1048592 | tf_op jit(solution)/shard_map/all_gather | solution.py:87
  394.8 2.3 copy.49
  397.0 38.8 %all-gather.13.cloned.1.call-done = bf16[2048,256]{0,1:T(8,128)(2,1)} async-done(((bf16[256,256]{0,1:T(8,128)(2,1)}), bf16[2048,256]{0,1:T(8,128)(2,1)}) %all-gather.13.cloned.1.call-update) | async-done | bytes 1048592 | tf_op jit(solution)/shard_map/all_gather | solution.py:86
  435.8 2.3 copy.48
  (81 shorter events, 32.9 us)
Async XLA Ops:
  7.2 46.0 %all-gather.7.cloned.1.call-start = ((), (), s32[]{:S(2)}) async-start(), calls=%async_computation.1 | async-start | bytes 1179648 | tf_op jit(solution)/shard_map/all_gather | solution.py:54
  7.9 86.4 %all-gather.9.cloned.1.call-start = ((), (), s32[]{:S(2)}) async-start(), calls=%async_computation.2 | async-start | bytes 1179648 | tf_op jit(solution)/shard_map/all_gather | solution.py:55
  8.7 126.8 %all-gather.11.cloned.1.call-start = ((), (), s32[]{:S(2)}) async-start(), calls=%async_computation.3 | async-start | bytes 1179648 | tf_op jit(solution)/shard_map/all_gather | solution.py:56
  9.4 5.9 %copy-start.11 = (bf16[2048,256]{1,0:T(8,128)(2,1)S(1)}, bf16[2048,256]{1,0:T(8,128)(2,1)}, u32[]{:S(2)}) copy-start(bf16[2048,256]{1,0:T(8,128)(2,1)} %param.17) | copy-start | bytes 3145732
  9.4 193.5 %reduce-scatter.4.cloned.1.call-start = ((), (), s32[]{:S(2)}) async-start(), calls=%async_computation.7 | async-start | bytes 884736
  15.3 5.9 %copy-start.10 = (bf16[2048,2048]{1,0:T(8,128)(2,1)S(1)}, bf16[2048,2048]{1,0:T(8,128)(2,1)}, u32[]{:S(2)}) copy-start(bf16[2048,2048]{1,0:T(8,128)(2,1)} %param.18) | copy-start | bytes 25165828
  15.3 6.1 %copy-start.12 = (bf16[2048,256]{1,0:T(8,128)(2,1)S(1)}, bf16[2048,256]{1,0:T(8,128)(2,1)}, u32[]{:S(2)}) copy-start(bf16[2048,256]{1,0:T(8,128)(2,1)} %param.15) | copy-start | bytes 3145732
  53.2 43.2 %copy-start.13 = (bf16[2048,256]{1,0:T(8,128)(2,1)S(1)}, bf16[2048,256]{1,0:T(8,128)(2,1)}, u32[]{:S(2)}) copy-start(bf16[2048,256]{1,0:T(8,128)(2,1)} %all-gather.7.cloned.1.call-done) | copy-start | bytes 3145732
  94.3 3.8 copy-start.14
  140.8 213.4 %all-gather.17.cloned.1.call-start = ((), (), s32[]{:S(2)}) async-start(), calls=%async_computation.6 | async-start | bytes 1179648 | tf_op jit(solution)/shard_map/all_gather | solution.py:88
  245.7 8.8 %collective-permute-start = (bf16[32,768]{0,1:T(8,128)(2,1)S(1)}, bf16[32,768]{0,1:T(8,128)(2,1)S(1)}, u32[]{:S(2)}, u32[]{:S(2)}) collective-permute-start(bf16[32,768]{0,1:T(8,128)(2,1)S(1)} %get-tuple-element.28), channel_id=1, source_target_pairs={{0,4},{4,8},{8,12},{12,16},{16,20},{20,24},{24,28},{28,0},{1,5},{5... | collective-permute-start | bytes 147464 | tf_op jit(solution)/shard_map/ppermute | solution.py:73
  254.5 8.4 %collective-permute-start.1 = (bf16[32,768]{0,1:T(8,128)(2,1)S(1)}, bf16[32,768]{0,1:T(8,128)(2,1)S(1)}, u32[]{:S(2)}, u32[]{:S(2)}) collective-permute-start(bf16[32,768]{0,1:T(8,128)(2,1)S(1)} %collective-permute-done), channel_id=1, source_target_pairs={{0,4},{4,8},{8,12},{12,16},{16,20},{20,24},{24,28},{28,0},{1,5},{5... | collective-permute-start | bytes 147464 | tf_op jit(solution)/shard_map/ppermute | solution.py:73
  262.9 8.4 %collective-permute-start.2 = (bf16[32,768]{0,1:T(8,128)(2,1)S(1)}, bf16[32,768]{0,1:T(8,128)(2,1)S(1)}, u32[]{:S(2)}, u32[]{:S(2)}) collective-permute-start(bf16[32,768]{0,1:T(8,128)(2,1)S(1)} %collective-permute-done.1), channel_id=1, source_target_pairs={{0,4},{4,8},{8,12},{12,16},{16,20},{20,24},{24,28},{28,0},{1,5},{5... | collective-permute-start | bytes 147464 | tf_op jit(solution)/shard_map/ppermute | solution.py:73
  271.2 28.2 %copy-start.2 = (bf16[32,768]{0,1:T(8,128)(2,1)}, bf16[32,768]{0,1:T(8,128)(2,1)S(1)}, u32[]{:S(2)}) copy-start(bf16[32,768]{0,1:T(8,128)(2,1)S(1)} %collective-permute-done.2) | copy-start | bytes 147460
  271.2 8.4 %collective-permute-start.3 = (bf16[32,768]{0,1:T(8,128)(2,1)S(1)}, bf16[32,768]{0,1:T(8,128)(2,1)S(1)}, u32[]{:S(2)}, u32[]{:S(2)}) collective-permute-start(bf16[32,768]{0,1:T(8,128)(2,1)S(1)} %collective-permute-done.2), channel_id=1, source_target_pairs={{0,4},{4,8},{8,12},{12,16},{16,20},{20,24},{24,28},{28,0},{1,5},{5... | collective-permute-start | bytes 147464 | tf_op jit(solution)/shard_map/ppermute | solution.py:73
  279.6 21.0 %copy-start.3 = (bf16[32,768]{0,1:T(8,128)(2,1)}, bf16[32,768]{0,1:T(8,128)(2,1)S(1)}, u32[]{:S(2)}) copy-start(bf16[32,768]{0,1:T(8,128)(2,1)S(1)} %collective-permute-done.3) | copy-start | bytes 147460
  279.6 9.3 %collective-permute-start.4 = (bf16[32,768]{0,1:T(8,128)(2,1)S(1)}, bf16[32,768]{0,1:T(8,128)(2,1)S(1)}, u32[]{:S(2)}, u32[]{:S(2)}) collective-permute-start(bf16[32,768]{0,1:T(8,128)(2,1)S(1)} %collective-permute-done.3), channel_id=1, source_target_pairs={{0,4},{4,8},{8,12},{12,16},{16,20},{20,24},{24,28},{28,0},{1,5},{5... | collective-permute-start | bytes 147464 | tf_op jit(solution)/shard_map/ppermute | solution.py:73
  288.9 11.7 %copy-start.4 = (bf16[32,768]{0,1:T(8,128)(2,1)}, bf16[32,768]{0,1:T(8,128)(2,1)S(1)}, u32[]{:S(2)}) copy-start(bf16[32,768]{0,1:T(8,128)(2,1)S(1)} %collective-permute-done.4) | copy-start | bytes 147460
  288.9 10.5 %collective-permute-start.5 = (bf16[32,768]{0,1:T(8,128)(2,1)S(1)}, bf16[32,768]{0,1:T(8,128)(2,1)S(1)}, u32[]{:S(2)}, u32[]{:S(2)}) collective-permute-start(bf16[32,768]{0,1:T(8,128)(2,1)S(1)} %collective-permute-done.4), channel_id=1, source_target_pairs={{0,4},{4,8},{8,12},{12,16},{16,20},{20,24},{24,28},{28,0},{1,5},{5... | collective-permute-start | bytes 147464 | tf_op jit(solution)/shard_map/ppermute | solution.py:73
  299.4 8.5 %collective-permute-start.6 = (bf16[32,768]{0,1:T(8,128)(2,1)S(1)}, bf16[32,768]{0,1:T(8,128)(2,1)}, u32[]{:S(2)}, u32[]{:S(2)}) collective-permute-start(bf16[32,768]{0,1:T(8,128)(2,1)S(1)} %collective-permute-done.5), channel_id=1, source_target_pairs={{0,4},{4,8},{8,12},{12,16},{16,20},{20,24},{24,28},{28,0},{1,5},{5... | collective-permute-start | bytes 147464 | tf_op jit(solution)/shard_map/ppermute | solution.py:73
  311.1 7.9 %copy-start.6 = (bf16[256,256]{1,0:T(8,128)(2,1)S(1)}, bf16[256,256]{1,0:T(8,128)(2,1)}, u32[]{:S(2)}) copy-start(bf16[256,256]{1,0:T(8,128)(2,1)} %param.22) | copy-start | bytes 393220
  312.3 5.6 %copy-start.1 = (f32[256,256]{1,0:T(8,128)}, f32[256,256]{1,0:T(8,128)S(1)}, u32[]{:S(2)}) copy-start(f32[256,256]{1,0:T(8,128)S(1)} %fusion.14) | copy-start | bytes 786436
  314.8 80.0 %all-gather.15.cloned.1.call-start = ((), (), s32[]{:S(2)}) async-start(), calls=%async_computation.5 | async-start | bytes 1179648 | tf_op jit(solution)/shard_map/all_gather | solution.py:87
  317.9 118.0 %all-gather.13.cloned.1.call-start = ((), (), s32[]{:S(2)}) async-start(), calls=%async_computation.4 | async-start | bytes 1179648 | tf_op jit(solution)/shard_map/all_gather | solution.py:86
  (5 other events, 13.6 us)
Sparse Core Ops, SparseCore 0:
  10.1 42.9 all-gather.6
  55.3 38.9 all-gather.8
  96.4 38.9 all-gather.10
  140.9 61.9 reduce-scatter.3
  314.9 39.1 all-gather.16
  356.6 38.0 all-gather.14
  397.4 38.3 all-gather.12
